TPU v7x, 32 devices: a whole 2x2x4 slice. The times are simulated.
32 devices in a mesh: sp: 16 (over z, y, x), tp: 2 (over core).
Axes of the slice: x: 2, y: 2, z: 4, core: 2. Of those that a mesh axis runs over, the one named last changes fastest.
Arguments:
- queries: bfloat16 [4096, 1024], P('sp', 'tp'), may hold values from -100 to 100
- keys: bfloat16 [256, 4096], P('tp', 'sp'), may hold values from -5 to 5
- values: bfloat16 [256, 4096], P('tp', 'sp'), may hold values from -4.5 to 4.5
- gate_cache: float32 [8, 4096], P('tp', 'sp'), as said below
- documents: int32 [4096], P('sp'), may hold values from 0 to 2, never falling along the last dimension, each value on 1 to 2560 neighbouring positions
- residual: bfloat16 [4096, 2048], P(('sp', 'tp')), may hold values from -3 to 3
- out_weight: bfloat16 [1024, 2048], replicated, may hold values from -2 to 2
- mix_gain: bfloat16 [2048], replicated, may hold values from 0.099609375 to 1.8984375
- routes: int32 [4096, 4], P(('sp', 'tp')), may hold values from 0 to 31, all different within a row; in each aligned block of 128 rows (0 to 127, 128 to 255, ...) at most 32 rows name the same one
- route_weight: float32 [4096, 4], P(('sp', 'tp')), may hold values from 0.25 to 1
- expert_gate: bfloat16 [32, 2048, 512], P(('sp', 'tp')), may hold values from -0.125 to 0.125
- expert_up: bfloat16 [32, 2048, 512], P(('sp', 'tp')), may hold values from -0.125 to 0.125
- expert_down: bfloat16 [32, 512, 2048], P(('sp', 'tp')), may hold values from -0.25 to 0.25
- shared_gate: bfloat16 [2048, 512], replicated, may hold values from -0.125 to 0.125
- shared_up: bfloat16 [2048, 512], replicated, may hold values from -0.125 to 0.125
- shared_down: bfloat16 [512, 2048], replicated, may hold values from -0.25 to 0.25
- ffn_gain: bfloat16 [2048], replicated, may hold values from 0.099609375 to 1.8984375
Outputs:
- result: bfloat16 [4096, 2048], P(('sp', 'tp'))
Inputs may be any that keep to these rules, and one draw needn't show every extreme that they name: `gate_cache`: entry (h, j) is the sum of head h's log forget gates over positions 0 to j. `documents`: never falls along the positions; no document has more than 2560 positions. `routes`: each row names 4 different experts; in the rows of one device (aligned blocks of 128 rows) no expert is named more than 32 times, a bound that some block reaches.
All inputs are finite; a program needn't handle non-finite values.
Results may differ from a plain program's by a relative error of at most 0.013.
Values may be sent and summed in bfloat16 or wider, within the bound.
A program may use at most 256 MiB of HBM per device.

v0:
```python
import jax
import jax.numpy as jnp
from jax import lax
from jax.sharding import PartitionSpec as P

HD = 128
residual_scale = 2.0**0.25
norm_epsilon = 1e-05
masked_score = -1e30


def normalize(summed, gain_vector):
    row_mean = jnp.mean(summed, axis=-1, keepdims=True)
    centred = summed - row_mean
    spread = jnp.mean(centred * centred, axis=-1, keepdims=True)
    return (centred * lax.rsqrt(spread + norm_epsilon) * gain_vector.astype(jnp.float32)).astype(
        jnp.bfloat16
    )


def expert_block(arrived, expert_gate, expert_up, expert_down):
    own_count = expert_gate.shape[0]
    grouped = arrived.reshape(-1, own_count, arrived.shape[1], arrived.shape[2])
    gate_part = jnp.einsum(
        "nemd,edf->nemf", grouped, expert_gate, preferred_element_type=jnp.float32
    )
    up_part = jnp.einsum("nemd,edf->nemf", grouped, expert_up, preferred_element_type=jnp.float32)
    hidden = (jax.nn.silu(gate_part) * up_part).astype(jnp.bfloat16)
    produced = jnp.einsum("nemf,efd->nemd", hidden, expert_down, preferred_element_type=jnp.float32)
    return produced.astype(jnp.bfloat16).reshape(arrived.shape)


def local(
    queries,
    keys,
    values,
    gate_cache,
    documents,
    residual,
    out_weight,
    mix_gain,
    routes,
    route_weight,
    expert_gate,
    expert_up,
    expert_down,
    shared_gate,
    shared_up,
    shared_down,
    ffn_gain,
):
    tok_rows = queries.shape[0]
    local_heads = gate_cache.shape[0]
    kv_local = keys.shape[0] // HD
    group_size = local_heads // kv_local
    score_scale = HD ** (-0.5)
    seq_start = lax.axis_index("sp") * tok_rows
    query_pos = seq_start + jnp.arange(tok_rows, dtype=jnp.int32)
    query_last = seq_start + tok_rows - 1
    query_cum = jnp.transpose(gate_cache).reshape(tok_rows, kv_local, group_size)
    grouped_q = queries.reshape(tok_rows, kv_local, group_size, HD)
    all_cache, all_docs = (
        lax.all_gather(gate_cache, "sp", axis=1, tiled=True),
        lax.all_gather(documents.reshape(1, tok_rows), "sp", axis=1, tiled=True),
    )
    doc_line = all_docs[0]
    initial = (
        jnp.full((tok_rows, kv_local, group_size), masked_score, jnp.float32),
        jnp.zeros((tok_rows, kv_local, group_size), jnp.float32),
        jnp.zeros((tok_rows, kv_local, group_size, HD), jnp.float32),
    )
    key_piece = lax.all_gather(keys, "sp", axis=1, tiled=True)
    value_piece = lax.all_gather(values, "sp", axis=1, tiled=True)
    width_keys = key_piece.shape[1]
    key_cum = all_cache.reshape(kv_local, group_size, width_keys)

    def update(state):
        running_max, running_sum, numerator = state
        key_block = key_piece.reshape(kv_local, HD, width_keys)
        value_block = value_piece.reshape(kv_local, HD, width_keys)
        scores = (
            jnp.einsum("qagd,adk->qagk", grouped_q, key_block, preferred_element_type=jnp.float32)
            * score_scale
        )
        scores = scores + query_cum[..., None] - key_cum[None]
        key_pos = jnp.arange(width_keys, dtype=jnp.int32)
        allowed = (key_pos[None, :] <= query_pos[:, None]) & (
            doc_line[None, :] == documents[:, None]
        )
        allowed = allowed[:, None, None, :]
        scores = jnp.where(allowed, scores, masked_score)
        new_max = jnp.maximum(running_max, jnp.max(scores, axis=-1))
        weights = jnp.where(allowed, jnp.exp(scores - new_max[..., None]), 0.0)
        new_sum = jnp.sum(weights, axis=-1)
        added = jnp.einsum(
            "qagk,adk->qagd",
            weights.astype(jnp.bfloat16),
            value_block,
            preferred_element_type=jnp.float32,
        )
        return (new_max, new_sum, added)

    active = (jnp.int32(0) <= query_last) & (doc_line[width_keys - 1] >= documents[0])
    running_max, running_sum, numerator = lax.cond(active, update, lambda state: state, initial)
    attended = (
        (numerator / running_sum[..., None])
        .astype(jnp.bfloat16)
        .reshape(tok_rows, local_heads * HD)
    )
    token_heads = lax.all_to_all(attended, "tp", split_axis=0, concat_axis=1, tiled=True)
    mixed = jnp.dot(token_heads, out_weight, preferred_element_type=jnp.float32)
    mixed = lax.optimization_barrier(mixed.astype(jnp.bfloat16)).astype(jnp.float32)
    settled = normalize(residual_scale * residual.astype(jnp.float32) + mixed, mix_gain)
    row_count = settled.shape[0]
    width_model = settled.shape[1]
    top_count = routes.shape[1]
    expert_total = lax.axis_size(("sp", "tp")) * expert_gate.shape[0]
    capacity = row_count * lax.axis_size("tp") * top_count // expert_total
    chosen_experts = routes.reshape(-1)
    matches = (
        chosen_experts[:, None] == jnp.arange(expert_total, dtype=jnp.int32)[None, :]
    ).astype(jnp.int32)
    ranks = jnp.sum(jnp.cumsum(matches, axis=0) * matches, axis=1) - 1
    slots = chosen_experts * capacity + ranks
    placing = slots[None, :] == jnp.arange(expert_total * capacity, dtype=jnp.int32)[:, None]
    placing = jnp.any(
        placing.reshape(expert_total * capacity, row_count, top_count), axis=2
    ).astype(jnp.bfloat16)
    outgoing = jnp.dot(placing, settled, preferred_element_type=jnp.float32).astype(jnp.bfloat16)
    outgoing = outgoing.reshape(expert_total, capacity, width_model)
    finished = expert_block(
        lax.all_to_all(outgoing, ("sp", "tp"), split_axis=0, concat_axis=0, tiled=True),
        expert_gate,
        expert_up,
        expert_down,
    )
    returned = lax.all_to_all(finished, ("sp", "tp"), split_axis=0, concat_axis=0, tiled=True)
    returned = returned.reshape(expert_total * capacity, width_model)
    picked_rows = jnp.take(returned, slots, axis=0).reshape(row_count, top_count, width_model)
    routed = jnp.einsum("rkd,rk->rd", picked_rows.astype(jnp.float32), route_weight)
    shared_gate_part = jnp.dot(settled, shared_gate, preferred_element_type=jnp.float32)
    shared_up_part = jnp.dot(settled, shared_up, preferred_element_type=jnp.float32)
    shared_hidden = (jax.nn.silu(shared_gate_part) * shared_up_part).astype(jnp.bfloat16)
    shared = jnp.dot(shared_hidden, shared_down, preferred_element_type=jnp.float32)
    return normalize(residual_scale * settled.astype(jnp.float32) + routed + shared, ffn_gain)


def solution(mesh):
    placed = (
        P("sp", "tp"),
        P("tp", "sp"),
        P("tp", "sp"),
        P("tp", "sp"),
        P("sp"),
        P(("sp", "tp"), None),
        P(),
        P(),
        P(("sp", "tp"), None),
        P(("sp", "tp"), None),
        P(("sp", "tp"), None, None),
        P(("sp", "tp"), None, None),
        P(("sp", "tp"), None, None),
        P(),
        P(),
        P(),
        P(),
    )
    return jax.shard_map(
        local, mesh=mesh, in_specs=placed, out_specs=P(("sp", "tp"), None), check_vma=False
    )
```

profile of v0, /device:TPU:0, one launch (start us, length us, event | category | flops | bytes accessed | tf_op | source)
XLA Modules:
  0.0 393.6 jit_solution(2535516395564024456)
XLA Ops:
  6.5 1.7 copy.56
  8.3 0.7 all-gather.7.cloned.1.call-update
  9.0 0.8 copy.59
  9.8 0.1 eq.59
  9.9 0.1 reshape.234
  10.1 1.2 slice.14
  11.3 42.7 %all-gather.1 = s32[16,1,256]{2,1,0:T(1,128)S(1)} all-gather(s32[1,1,256]{2,1,0:T(1,128)} %bitcast.172), channel_id=2, replica_groups=mesh['sp'=16,'tp'=2] {'sp'}, dimensions={0}, use_global_device_ids=true | all-gather | bytes 17408 | tf_op jit(solution)/shard_map/all_gather | solution.py:64
  54.0 0.6 slice.19
  55.8 0.7 convert_element_type.60
  56.5 1.2 reduce-window.6
  57.7 0.2 slice_reduce_fusion
  58.0 0.1 fusion.50
  58.1 0.1 sub.47
  58.3 36.1 %all_gather.14 = f32[4,4096]{1,0:T(4,128)S(1)} all-gather(f32[4,256]{1,0:T(4,128)} %param.22), channel_id=1, replica_groups=mesh['sp'=16,'tp'=2] {'sp'}, dimensions={1}, use_global_device_ids=true | all-gather | bytes 69632 | tf_op jit(solution)/shard_map/all_gather | solution.py:63
  94.4 0.7 compare_and_fusion
  95.1 0.4 fusion.31
  95.4 29.3 %all-gather.7.cloned.1.call-done = bf16[128,4096]{1,0:T(8,128)(2,1)} async-done(((bf16[128,256]{1,0:T(8,128)(2,1)}), bf16[128,4096]{1,0:T(8,128)(2,1)}) %all-gather.7.cloned.1.call-update) | async-done | bytes 1048592 | tf_op jit(solution)/shard_map/all_gather | solution.py:73
  124.7 20.7 %conditional.1 = (f32[256,1,4]{0,2,1:T(4,128)S(1)}, f32[256,1,4,128]{3,0,2,1:T(8,128)S(1)}) conditional(s32[]{:T(128)} %convert_element_type.56, () %tuple.13, (s32[]{:T(128)}, s32[256]{0:T(256)S(1)}, s32[1,4096]{1,0:T(1,128)S(1)}, s32[256]{0:T(256)}, bf16[256,512]{1,0:T(8,128)(2,1)}, /*index=5*/bf16[128,4096]{0,1:T(8,128)(2,1)}, f32[256,4]{0,1:T(4,128)}, ...), branch_computations={%region_0.0_spmd, %region_1.4_spmd} | conditional | flops 2230320384 | bytes 61874252 | solution.py:104
  124.7 2.5 fusion.8
  127.3 5.5 %fusion.3 = (f32[256,4]{0,1:T(4,128)S(1)}, f32[4096,256,4]{1,0,2:T(8,128)S(1)}) fusion(f32[4,4096]{1,0:T(4,128)S(1)} %get-tuple-element.33, f32[256,4]{0,1:T(4,128)} %get-tuple-element.32, pred[256,4096]{0,1:T(8,128)(4,1)S(1)} %fusion.8, bf16[128,4096]{0,1:T(8,128)(2,1)} %get-tuple-element.30, bf16[256,512]{1,0:T(8,128)(2,1)} %get-tuple-element.40), kind=kOutput, calls=%fused_computation.7 | convolution fusion | flops 1094712320 | bytes 19210240 | tf_op jit(solution)/shard_map/cond/branch_1_fun/qagd,adk->qagk/dot_general | solution.py:82
  132.8 6.8 %fusion.9 = f32[256,1,4,128]{3,0,2,1:T(8,128)S(1)} fusion(f32[4096,256,4]{1,0,2:T(8,128)S(1)} %get-tuple-element.44, f32[256,4]{0,1:T(4,128)S(1)} %broadcast_maximum_fusion, f32[4,4096]{1,0:T(4,128)S(1)} %get-tuple-element.33, f32[256,4]{0,1:T(4,128)S(1)} %copy-done.5, pred[256,4096]{0,1:T(8,128)(4,1)S(1)} %fusion.8, bf16[128,4096]{1,0:T(8,128)(2,1)S(1)} %copy-done.9), kind=kOutput, calls=%fused_computation.13 | convolution fusion | flops 1103101952 | bytes 19472384 | tf_op jit(solution)/shard_map/cond/branch_1_fun/qagk,adk->qagd/dot_general | solution.py:95
  139.7 5.8 %fusion.2 = f32[256,4]{0,1:T(4,128)S(1)} fusion(f32[4096,256,4]{1,0,2:T(8,128)S(1)} %get-tuple-element.44, f32[256,4]{0,1:T(4,128)S(1)} %broadcast_maximum_fusion, f32[4,4096]{1,0:T(4,128)S(1)} %get-tuple-element.33, f32[256,4]{0,1:T(4,128)S(1)} %copy-done.5, pred[256,4096]{0,1:T(8,128)(4,1)S(1)} %fusion.8), kind=kLoop, calls=%fused_computation.6 | loop fusion | flops 29359104 | bytes 17903616 | tf_op jit(solution)/shard_map/cond/branch_1_fun/reduce_sum | solution.py:94
  145.5 0.2 divide_convert_fusion
  145.7 0.2 copy.57
  146.0 3.9 %all_to_all.29 = bf16[2,128,512]{2,1,0:T(8,128)(2,1)S(1)} all-to-all(bf16[2,128,512]{2,1,0:T(8,128)(2,1)S(1)} %all_to_all.20), channel_id=1, replica_groups=mesh['sp'=16,'tp'=2] {'tp'}, dimensions={0} | all-to-all | bytes 524288 | tf_op jit(solution)/shard_map/all_to_all | solution.py:110
  149.9 0.2 copy.58
  150.1 2.9 convolution_convert_fusion.2
  153.1 0.3 fusion.40
  153.3 0.3 multiply_reduce_fusion.1
  153.7 0.3 multiply_convert_fusion.1
  154.0 1.2 convolution_convert_fusion.1
  155.2 96.7 %all_to_all.30 = bf16[32,32,2048]{2,1,0:T(8,128)(2,1)S(1)} all-to-all(bf16[32,32,2048]{2,1,0:T(8,128)(2,1)S(1)} %bitcast.161), channel_id=1, replica_groups=mesh['sp'=16,'tp'=2] {'sp','tp'}, dimensions={0} | all-to-all | bytes 8388608 | tf_op jit(solution)/shard_map/all_to_all | solution.py:132
  252.0 2.0 copy-done.3
  253.9 3.7 fusion.22
  257.7 10.1 %convolution_convert_fusion = bf16[32,32,2048]{2,1,0:T(8,128)(2,1)} fusion(bf16[1,512,2048]{2,1,0:T(8,128)(2,1)S(1)} %copy-done, f32[32,32,512]{2,1,0:T(8,128)} %fusion.22, bf16[32,32,2048]{2,1,0:T(8,128)(2,1)} %copy-done.3, bf16[1,2048,512]{2,1,0:T(8,128)(2,1)} %param.29), kind=kOutput, calls=%fused_computation.24 | convolution fusion | flops 4300210176 | bytes 14680064 | tf_op jit(solution)/shard_map/nemf,efd->nemd/dot_general | solution.py:29
  267.7 4.0 %all-to-all-start.2 = ((bf16[32,32,2048]{2,1,0:T(8,128)(2,1)}), bf16[32,32,2048]{2,1,0:T(8,128)(2,1)}, u32[]{:S(2)}, u32[]{:S(2)}) async-start(bf16[32,32,2048]{2,1,0:T(8,128)(2,1)} %convolution_convert_fusion), calls=%async_computation.2 | async-start | bytes 8388608 | tf_op jit(solution)/shard_map/all_to_all | solution.py:137
  271.8 0.1 copy.64
  271.9 0.1 mul.107
  272.0 0.1 copy.63
  272.2 0.2 copy.66
  272.4 2.0 fusion.58
  274.4 91.0 %all-to-all-done.2 = bf16[32,32,2048]{2,1,0:T(8,128)(2,1)} async-done(((bf16[32,32,2048]{2,1,0:T(8,128)(2,1)}), bf16[32,32,2048]{2,1,0:T(8,128)(2,1)}, u32[]{:S(2)}, u32[]{:S(2)}) %all-to-all-start.2) | async-done | bytes 4194336 | tf_op jit(solution)/shard_map/all_to_all | solution.py:137
  365.5 8.0 %gather_fusion = bf16[512,2048]{1,0:T(8,128)(2,1)} fusion(bf16[1024,2048]{1,0:T(8,128)(2,1)} %bitcast.35, s32[1024]{0:T(1024)S(1)} %pad_clamp_fusion), kind=kCustom, calls=%fused_computation | custom fusion | bytes 4196352 | tf_op jit(solution)/shard_map/jit(_take)/gather | solution.py:139
  373.5 4.1 %gather.7 = bf16[128,4,2048]{2,1,0:T(4,128)(2,1)} reshape(bf16[512,2048]{1,0:T(8,128)(2,1)} %gather_fusion) | data formatting | bytes 4194304 | tf_op jit(solution)/shard_map/jit(_take)/gather | solution.py:139
  377.6 3.9 fusion.29
  381.5 4.0 %fusion.57 = (f32[128]{0:T(128)S(1)}, f32[128,2048]{1,0:T(8,128)S(1)}) fusion(bf16[512,2048]{1,0:T(8,128)(2,1)} %param.34, bf16[128,2048]{1,0:T(8,128)(2,1)} %copy-done.1, bf16[2048,512]{1,0:T(8,128)(2,1)} %param.33, f32[128,512]{1,0:T(8,128)S(1)} %fusion.58, f32[128,1,2048]{2,1,0:T(1,128)} %fusion.29), kind=kOutput, calls=%fused_computation.85 | convolution fusion | flops 538574720 | bytes 7078400 | tf_op jit(solution)/shard_map/dot_general | solution.py:144
  385.5 0.3 multiply_reduce_fusion
  385.7 1.0 multiply_convert_fusion
  (40 shorter events, 0.4 us)
Async XLA Ops:
  6.5 251.1 %copy-start = (bf16[1,512,2048]{2,1,0:T(8,128)(2,1)S(1)}, bf16[1,512,2048]{2,1,0:T(8,128)(2,1)}, u32[]{:S(2)}) copy-start(bf16[1,512,2048]{2,1,0:T(8,128)(2,1)} %param.31) | copy-start | bytes 6291460
  6.5 88.9 %all-gather.5.cloned.1.call-start = ((), (), s32[]{:S(2)}) async-start(), calls=%async_computation.3 | async-start | bytes 1114112 | tf_op jit(solution)/shard_map/all_gather | solution.py:72
  8.3 116.4 %all-gather.7.cloned.1.call-start = ((), (), s32[]{:S(2)}) async-start(), calls=%async_computation.4 | async-start | bytes 1114112 | tf_op jit(solution)/shard_map/all_gather | solution.py:73
  127.3 5.5 %copy-start.5 = (f32[256,4]{0,1:T(4,128)S(1)}, f32[256,4]{0,1:T(4,128)}, u32[]{:S(2)}) copy-start(f32[256,4]{0,1:T(4,128)} %get-tuple-element.32) | copy-start | bytes 12292 | tf_op jit(solution)/shard_map/cond
  127.3 5.5 %copy-start.9 = (bf16[128,4096]{1,0:T(8,128)(2,1)S(1)}, bf16[128,4096]{1,0:T(8,128)(2,1)}, u32[]{:S(2)}) copy-start(bf16[128,4096]{1,0:T(8,128)(2,1)} %get-tuple-element.34) | copy-start | bytes 3145732 | tf_op jit(solution)/shard_map/cond
  145.5 7.6 %copy-start.2 = (bf16[128,2048]{1,0:T(8,128)(2,1)S(1)}, bf16[128,2048]{1,0:T(8,128)(2,1)}, u32[]{:S(2)}) copy-start(bf16[128,2048]{1,0:T(8,128)(2,1)} %param.24) | copy-start | bytes 1572868
  154.0 118.4 %copy-start.1 = (bf16[128,2048]{1,0:T(8,128)(2,1)}, bf16[128,2048]{1,0:T(8,128)(2,1)S(1)}, u32[]{:S(2)}) copy-start(bf16[128,2048]{1,0:T(8,128)(2,1)S(1)} %multiply_convert_fusion.1) | copy-start | bytes 1572868
  155.2 98.7 %copy-start.8 = (bf16[1,2048,512]{2,1,0:T(8,128)(2,1)S(1)}, bf16[1,2048,512]{2,1,0:T(8,128)(2,1)}, u32[]{:S(2)}) copy-start(bf16[1,2048,512]{2,1,0:T(8,128)(2,1)} %param.30) | copy-start | bytes 6291460
  252.0 2.0 copy-start.3
  267.7 4.0 %copy-start.4 = (s32[128,4]{0,1:T(4,128)S(1)}, s32[128,4]{0,1:T(4,128)}, u32[]{:S(2)}) copy-start(s32[128,4]{0,1:T(4,128)} %param.27) | copy-start | bytes 6148
  267.7 4.4 %copy-start.7 = (f32[128,4]{0,1:T(4,128)S(1)}, f32[128,4]{0,1:T(4,128)}, u32[]{:S(2)}) copy-start(f32[128,4]{0,1:T(4,128)} %param.28) | copy-start | bytes 6148
  267.7 4.6 %copy-start.6 = (bf16[2048]{0:T(1024)(128)(2,1)S(1)}, bf16[2048]{0:T(1024)(128)(2,1)}, u32[]{:S(2)}) copy-start(bf16[2048]{0:T(1024)(128)(2,1)} %param.35) | copy-start | bytes 12292
  267.7 97.7 %all-to-all-start.2 = ((bf16[32,32,2048]{2,1,0:T(8,128)(2,1)}), bf16[32,32,2048]{2,1,0:T(8,128)(2,1)}, u32[]{:S(2)}, u32[]{:S(2)}) async-start(bf16[32,32,2048]{2,1,0:T(8,128)(2,1)} %convolution_convert_fusion), calls=%async_computation.2 | async-start | bytes 8388608 | tf_op jit(solution)/shard_map/all_to_all | solution.py:137
Sparse Core Ops, SparseCore 0:
  10.1 57.9 all-gather.4
  70.8 53.9 all-gather.6
where the time goes:
time: 394 us
  blocking collectives  180 us (46%)
  waiting for transfers between devices  121 us (31%)
  matrix products  40.2 us (10%)
  local copies, waits for them, and re-layouts  20.1 us (5%)
  between operations  14.9 us (4%)
  other arithmetic  13.8 us (4%)
  starting transfers between devices  4.06 us (1%)
    all_to_all x1, blocking collectives, local(): lax.all_to_all(outgoing, ('sp', 'tp'), split_axis=0, concat_axis=0, tiled...  96.7 us
    all_to_all x1, waiting for transfers between devices, local(): lax.all_to_all(finished, ('sp', 'tp'), split_axis=0, concat_axis=0, tiled...  91 us
    all_gather x1, blocking collectives, local(): lax.all_gather(documents.reshape(1, tok_rows), 'sp', axis=1, tiled=True)  42.7 us
    all_gather x1, blocking collectives, local(): lax.all_gather(gate_cache, 'sp', axis=1, tiled=True)  36.1 us
    all_gather x1, waiting for transfers between devices, local(): value_piece = lax.all_gather(values, 'sp', axis=1, tiled=True)  29.3 us
    gather x2, local copies, waits for them, and re-layouts, local(): jnp.take(returned, slots, axis=0).reshape(row_count, top_count, width_model)  12.1 us
    dot_general x1, matrix products, expert_block(): jnp.einsum('nemf,efd->nemd', hidden, expert_down, preferred_element_type=...  10.1 us
  transfers between devices with their start and end apart: 3, of which 2 were waited for; matrix products, arithmetic and copies ran while one was open for 2% of the time, Pallas kernels for 0%

commit v1 on v0

--- a/solution.py
+++ b/solution.py
@@ -49,6 +49,12 @@
     shared_down,
     ffn_gain,
 ):
+
+    def number_task(u):
+        raw_out = jax.lax.all_gather(u, "sp")
+        built = jnp.concatenate(raw_out, axis=1)
+        return built
+
     tok_rows = queries.shape[0]
     local_heads = gate_cache.shape[0]
     kv_local = keys.shape[0] // HD
@@ -60,7 +66,7 @@
     query_cum = jnp.transpose(gate_cache).reshape(tok_rows, kv_local, group_size)
     grouped_q = queries.reshape(tok_rows, kv_local, group_size, HD)
     all_cache, all_docs = (
-        lax.all_gather(gate_cache, "sp", axis=1, tiled=True),
+        number_task(gate_cache),
         lax.all_gather(documents.reshape(1, tok_rows), "sp", axis=1, tiled=True),
     )
     doc_line = all_docs[0]

time: 394 us -> 394 us (level)
  no operation moved by 1% of the time
where the time goes in v1:
time: 394 us
  blocking collectives  180 us (46%)
  waiting for transfers between devices  121 us (31%)
  matrix products  40.2 us (10%)
  local copies, waits for them, and re-layouts  20.1 us (5%)
  between operations  14.9 us (4%)
  other arithmetic  13.8 us (4%)
  starting transfers between devices  4.06 us (1%)
    all_to_all x1, blocking collectives, local(): lax.all_to_all(outgoing, ('sp', 'tp'), split_axis=0, concat_axis=0, tiled...  96.7 us
    all_to_all x1, waiting for transfers between devices, local(): lax.all_to_all(finished, ('sp', 'tp'), split_axis=0, concat_axis=0, tiled...  91 us
    all_gather x1, blocking collectives, local(): lax.all_gather(documents.reshape(1, tok_rows), 'sp', axis=1, tiled=True)  42.7 us
    all_gather x1, blocking collectives, number_task(): raw_out = jax.lax.all_gather(u, 'sp')  36.1 us
    all_gather x1, waiting for transfers between devices, local(): value_piece = lax.all_gather(values, 'sp', axis=1, tiled=True)  29.3 us
    gather x2, local copies, waits for them, and re-layouts, local(): jnp.take(returned, slots, axis=0).reshape(row_count, top_count, width_model)  12.1 us
    dot_general x1, matrix products, expert_block(): jnp.einsum('nemf,efd->nemd', hidden, expert_down, preferred_element_type=...  10.1 us
  transfers between devices with their start and end apart: 3, of which 2 were waited for; matrix products, arithmetic and copies ran while one was open for 2% of the time, Pallas kernels for 0%

profile of v1, /device:TPU:0, one launch (start us, length us, event | category | flops | bytes accessed | tf_op | source)
XLA Modules:
  0.0 393.6 jit_solution(11205409485144801095)
XLA Ops:
  6.5 1.7 copy.58
  8.3 0.7 all-gather.9.cloned.1.call-update
  9.0 0.8 copy.62
  9.8 0.1 eq.59
  9.9 0.1 reshape.238
  10.1 1.2 slice.14
  11.3 42.7 %all-gather.2 = s32[16,1,256]{2,1,0:T(1,128)S(1)} all-gather(s32[1,1,256]{2,1,0:T(1,128)} %bitcast.180), channel_id=2, replica_groups=mesh['sp'=16,'tp'=2] {'sp'}, dimensions={0}, use_global_device_ids=true | all-gather | bytes 17408 | tf_op jit(solution)/shard_map/all_gather | solution.py:70
  54.0 0.6 slice.19
  55.8 0.7 convert_element_type.60
  56.5 1.2 reduce-window.6
  57.7 0.2 slice_reduce_fusion
  58.0 0.1 fusion.50
  58.1 0.1 sub.49
  58.3 36.1 %all-gather.3 = f32[16,4,256]{2,1,0:T(4,128)S(1)} all-gather(f32[1,4,256]{2,1,0:T(4,128)} %bitcast.175), channel_id=3, replica_groups=mesh['sp'=16,'tp'=2] {'sp'}, dimensions={0}, use_global_device_ids=true | all-gather | bytes 69632 | tf_op jit(solution)/shard_map/all_gather | solution.py:54
  94.4 0.7 compare_and_fusion
  95.1 0.4 fusion.31
  95.4 29.3 %all-gather.9.cloned.1.call-done = bf16[128,4096]{1,0:T(8,128)(2,1)} async-done(((bf16[128,256]{1,0:T(8,128)(2,1)}), bf16[128,4096]{1,0:T(8,128)(2,1)}) %all-gather.9.cloned.1.call-update) | async-done | bytes 1048592 | tf_op jit(solution)/shard_map/all_gather | solution.py:79
  124.7 20.7 %conditional.1 = (f32[256,1,4]{0,2,1:T(4,128)S(1)}, f32[256,1,4,128]{3,0,2,1:T(8,128)S(1)}) conditional(s32[]{:T(128)} %convert_element_type.56, () %tuple.13, (s32[]{:T(128)}, s32[256]{0:T(256)S(1)}, s32[1,4096]{1,0:T(1,128)S(1)}, s32[256]{0:T(256)}, bf16[256,512]{1,0:T(8,128)(2,1)}, /*index=5*/bf16[128,4096]{0,1:T(8,128)(2,1)}, f32[256,4]{0,1:T(4,128)}, ...), branch_computations={%region_0.0_spmd, %region_1.4_spmd} | conditional | flops 2230320384 | bytes 61874252 | solution.py:110
  124.7 2.5 fusion.8
  127.3 5.5 %fusion.3 = (f32[256,4]{0,1:T(4,128)S(1)}, f32[4096,256,4]{1,0,2:T(8,128)S(1)}) fusion(f32[4,4096]{1,0:T(4,128)S(1)} %bitcast.168, f32[256,4]{0,1:T(4,128)} %get-tuple-element.32, pred[256,4096]{0,1:T(8,128)(4,1)S(1)} %fusion.8, bf16[128,4096]{0,1:T(8,128)(2,1)} %get-tuple-element.30, bf16[256,512]{1,0:T(8,128)(2,1)} %get-tuple-element.40), kind=kOutput, calls=%fused_computation.7 | convolution fusion | flops 1094712320 | bytes 19210240 | tf_op jit(solution)/shard_map/cond/branch_1_fun/qagd,adk->qagk/dot_general | solution.py:88
  132.8 6.8 %fusion.9 = f32[256,1,4,128]{3,0,2,1:T(8,128)S(1)} fusion(f32[4096,256,4]{1,0,2:T(8,128)S(1)} %get-tuple-element.71, f32[256,4]{0,1:T(4,128)S(1)} %broadcast_maximum_fusion, f32[4,4096]{1,0:T(4,128)S(1)} %bitcast.169, f32[256,4]{0,1:T(4,128)S(1)} %copy-done.5, pred[256,4096]{0,1:T(8,128)(4,1)S(1)} %fusion.8, bf16[128,4096]{1,0:T(8,128)(2,1)S(1)} %copy-done.9), kind=kOutput, calls=%fused_computation.13 | convolution fusion | flops 1103101952 | bytes 19472384 | tf_op jit(solution)/shard_map/cond/branch_1_fun/qagk,adk->qagd/dot_general | solution.py:101
  139.7 5.8 %fusion.2 = f32[256,4]{0,1:T(4,128)S(1)} fusion(f32[4096,256,4]{1,0,2:T(8,128)S(1)} %get-tuple-element.71, f32[256,4]{0,1:T(4,128)S(1)} %broadcast_maximum_fusion, f32[4,4096]{1,0:T(4,128)S(1)} %bitcast.170, f32[256,4]{0,1:T(4,128)S(1)} %copy-done.5, pred[256,4096]{0,1:T(8,128)(4,1)S(1)} %fusion.8), kind=kLoop, calls=%fused_computation.6 | loop fusion | flops 29359104 | bytes 17903616 | tf_op jit(solution)/shard_map/cond/branch_1_fun/reduce_sum | solution.py:100
  145.5 0.2 divide_convert_fusion
  145.7 0.2 copy.60
  146.0 3.9 %all_to_all.29 = bf16[2,128,512]{2,1,0:T(8,128)(2,1)S(1)} all-to-all(bf16[2,128,512]{2,1,0:T(8,128)(2,1)S(1)} %all_to_all.20), channel_id=1, replica_groups=mesh['sp'=16,'tp'=2] {'tp'}, dimensions={0} | all-to-all | bytes 524288 | tf_op jit(solution)/shard_map/all_to_all | solution.py:116
  149.9 0.2 copy.61
  150.1 2.9 convolution_convert_fusion.2
  153.1 0.3 fusion.40
  153.3 0.3 multiply_reduce_fusion.1
  153.7 0.3 multiply_convert_fusion.1
  154.0 1.2 convolution_convert_fusion.1
  155.2 96.7 %all_to_all.30 = bf16[32,32,2048]{2,1,0:T(8,128)(2,1)S(1)} all-to-all(bf16[32,32,2048]{2,1,0:T(8,128)(2,1)S(1)} %bitcast.164), channel_id=1, replica_groups=mesh['sp'=16,'tp'=2] {'sp','tp'}, dimensions={0} | all-to-all | bytes 8388608 | tf_op jit(solution)/shard_map/all_to_all | solution.py:138
  252.0 2.0 copy-done.3
  253.9 3.7 fusion.22
  257.7 10.1 %convolution_convert_fusion = bf16[32,32,2048]{2,1,0:T(8,128)(2,1)} fusion(bf16[1,512,2048]{2,1,0:T(8,128)(2,1)S(1)} %copy-done, f32[32,32,512]{2,1,0:T(8,128)} %fusion.22, bf16[32,32,2048]{2,1,0:T(8,128)(2,1)} %copy-done.3, bf16[1,2048,512]{2,1,0:T(8,128)(2,1)} %param.29), kind=kOutput, calls=%fused_computation.24 | convolution fusion | flops 4300210176 | bytes 14680064 | tf_op jit(solution)/shard_map/nemf,efd->nemd/dot_general | solution.py:29
  267.7 4.0 %all-to-all-start.2 = ((bf16[32,32,2048]{2,1,0:T(8,128)(2,1)}), bf16[32,32,2048]{2,1,0:T(8,128)(2,1)}, u32[]{:S(2)}, u32[]{:S(2)}) async-start(bf16[32,32,2048]{2,1,0:T(8,128)(2,1)} %convolution_convert_fusion), calls=%async_computation.2 | async-start | bytes 8388608 | tf_op jit(solution)/shard_map/all_to_all | solution.py:143
  271.8 0.1 copy.67
  271.9 0.1 mul.107
  272.0 0.1 copy.66
  272.2 0.2 copy.69
  272.4 2.0 fusion.58
  274.4 91.0 %all-to-all-done.2 = bf16[32,32,2048]{2,1,0:T(8,128)(2,1)} async-done(((bf16[32,32,2048]{2,1,0:T(8,128)(2,1)}), bf16[32,32,2048]{2,1,0:T(8,128)(2,1)}, u32[]{:S(2)}, u32[]{:S(2)}) %all-to-all-start.2) | async-done | bytes 4194336 | tf_op jit(solution)/shard_map/all_to_all | solution.py:143
  365.5 8.0 %gather_fusion = bf16[512,2048]{1,0:T(8,128)(2,1)} fusion(bf16[1024,2048]{1,0:T(8,128)(2,1)} %bitcast.38, s32[1024]{0:T(1024)S(1)} %pad_clamp_fusion), kind=kCustom, calls=%fused_computation | custom fusion | bytes 4196352 | tf_op jit(solution)/shard_map/jit(_take)/gather | solution.py:145
  373.5 4.1 %gather.7 = bf16[128,4,2048]{2,1,0:T(4,128)(2,1)} reshape(bf16[512,2048]{1,0:T(8,128)(2,1)} %gather_fusion) | data formatting | bytes 4194304 | tf_op jit(solution)/shard_map/jit(_take)/gather | solution.py:145
  377.6 3.9 fusion.29
  381.5 4.0 %fusion.57 = (f32[128]{0:T(128)S(1)}, f32[128,2048]{1,0:T(8,128)S(1)}) fusion(bf16[512,2048]{1,0:T(8,128)(2,1)} %param.34, bf16[128,2048]{1,0:T(8,128)(2,1)} %copy-done.1, bf16[2048,512]{1,0:T(8,128)(2,1)} %param.33, f32[128,512]{1,0:T(8,128)S(1)} %fusion.58, f32[128,1,2048]{2,1,0:T(1,128)} %fusion.29), kind=kOutput, calls=%fused_computation.85 | convolution fusion | flops 538574720 | bytes 7078400 | tf_op jit(solution)/shard_map/dot_general | solution.py:150
  385.5 0.3 multiply_reduce_fusion
  385.7 1.0 multiply_convert_fusion
  (40 shorter events, 0.4 us)
Async XLA Ops:
  6.5 251.1 %copy-start = (bf16[1,512,2048]{2,1,0:T(8,128)(2,1)S(1)}, bf16[1,512,2048]{2,1,0:T(8,128)(2,1)}, u32[]{:S(2)}) copy-start(bf16[1,512,2048]{2,1,0:T(8,128)(2,1)} %param.31) | copy-start | bytes 6291460
  6.5 88.9 %all-gather.7.cloned.1.call-start = ((), (), s32[]{:S(2)}) async-start(), calls=%async_computation.3 | async-start | bytes 1114112 | tf_op jit(solution)/shard_map/all_gather | solution.py:78
  8.3 116.4 %all-gather.9.cloned.1.call-start = ((), (), s32[]{:S(2)}) async-start(), calls=%async_computation.4 | async-start | bytes 1114112 | tf_op jit(solution)/shard_map/all_gather | solution.py:79
  127.3 5.5 %copy-start.5 = (f32[256,4]{0,1:T(4,128)S(1)}, f32[256,4]{0,1:T(4,128)}, u32[]{:S(2)}) copy-start(f32[256,4]{0,1:T(4,128)} %get-tuple-element.32) | copy-start | bytes 12292 | tf_op jit(solution)/shard_map/cond
  127.3 5.5 %copy-start.9 = (bf16[128,4096]{1,0:T(8,128)(2,1)S(1)}, bf16[128,4096]{1,0:T(8,128)(2,1)}, u32[]{:S(2)}) copy-start(bf16[128,4096]{1,0:T(8,128)(2,1)} %get-tuple-element.34) | copy-start | bytes 3145732 | tf_op jit(solution)/shard_map/cond
  145.5 7.6 %copy-start.2 = (bf16[128,2048]{1,0:T(8,128)(2,1)S(1)}, bf16[128,2048]{1,0:T(8,128)(2,1)}, u32[]{:S(2)}) copy-start(bf16[128,2048]{1,0:T(8,128)(2,1)} %param.24) | copy-start | bytes 1572868
  154.0 118.4 %copy-start.1 = (bf16[128,2048]{1,0:T(8,128)(2,1)}, bf16[128,2048]{1,0:T(8,128)(2,1)S(1)}, u32[]{:S(2)}) copy-start(bf16[128,2048]{1,0:T(8,128)(2,1)S(1)} %multiply_convert_fusion.1) | copy-start | bytes 1572868
  155.2 98.7 %copy-start.8 = (bf16[1,2048,512]{2,1,0:T(8,128)(2,1)S(1)}, bf16[1,2048,512]{2,1,0:T(8,128)(2,1)}, u32[]{:S(2)}) copy-start(bf16[1,2048,512]{2,1,0:T(8,128)(2,1)} %param.30) | copy-start | bytes 6291460
  252.0 2.0 copy-start.3
  267.7 4.0 %copy-start.4 = (s32[128,4]{0,1:T(4,128)S(1)}, s32[128,4]{0,1:T(4,128)}, u32[]{:S(2)}) copy-start(s32[128,4]{0,1:T(4,128)} %param.27) | copy-start | bytes 6148
  267.7 4.4 %copy-start.7 = (f32[128,4]{0,1:T(4,128)S(1)}, f32[128,4]{0,1:T(4,128)}, u32[]{:S(2)}) copy-start(f32[128,4]{0,1:T(4,128)} %param.28) | copy-start | bytes 6148
  267.7 4.6 %copy-start.6 = (bf16[2048]{0:T(1024)(128)(2,1)S(1)}, bf16[2048]{0:T(1024)(128)(2,1)}, u32[]{:S(2)}) copy-start(bf16[2048]{0:T(1024)(128)(2,1)} %param.35) | copy-start | bytes 12292
  267.7 97.7 %all-to-all-start.2 = ((bf16[32,32,2048]{2,1,0:T(8,128)(2,1)}), bf16[32,32,2048]{2,1,0:T(8,128)(2,1)}, u32[]{:S(2)}, u32[]{:S(2)}) async-start(bf16[32,32,2048]{2,1,0:T(8,128)(2,1)} %convolution_convert_fusion), calls=%async_computation.2 | async-start | bytes 8388608 | tf_op jit(solution)/shard_map/all_to_all | solution.py:143
Sparse Core Ops, SparseCore 0:
  10.1 57.9 all-gather.6
  70.8 53.9 all-gather.8
